TPU v7x, 32 devices: a whole 2x2x4 slice. The times are simulated.
32 devices in a mesh: rep: 2 (over x), fs: 8 (over z, y), tp: 2 (over core).
Axes of the slice: x: 2, y: 2, z: 4, core: 2. Of those that a mesh axis runs over, the one named last changes fastest.
Arguments:
- tokens: bfloat16 [10240, 2048], P(('rep', 'fs', 'tp')), may hold values from -6 to 6
- mix_gain: float32 [2048], replicated, may hold values from 0.1 to 1.9
- w_bgate: bfloat16 [2048, 2048], P('fs', 'tp'), may hold values from -0.125 to 0.125
- w_cgate: bfloat16 [2048, 2048], P('fs', 'tp'), may hold values from -0.125 to 0.125
- w_value: bfloat16 [2048, 2048], P('fs', 'tp'), may hold values from -0.125 to 0.125
- conv_taps: float32 [3, 2048], replicated, may hold values from -3 to 3
- w_mixout: bfloat16 [2048, 2048], P('tp', 'fs'), may hold values from -0.125 to 0.125
- mlp_gain: float32 [2048], replicated, may hold values from 0.1 to 1.9
- w_gate: bfloat16 [2048, 2816], P('fs', 'tp'), may hold values from -0.125 to 0.125
- w_up: bfloat16 [2048, 2816], P('fs', 'tp'), may hold values from -0.125 to 0.125
- w_down: bfloat16 [2816, 2048], P('tp', 'fs'), may hold values from -0.109375 to 0.109375
Outputs:
- block_out: bfloat16 [10240, 2048], P(('rep', 'fs', 'tp'))
All inputs are finite; a program needn't handle non-finite values.
Results may differ from a plain program's by a relative error of at most 0.0085.
Values may be sent and summed in bfloat16 or wider, within the bound.
A program may use at most 128 MiB of HBM per device.

v0:
```python
import jax
import jax.numpy as jnp
from jax import lax
from jax.sharding import PartitionSpec as P


def rms_scale(matrix, gain):
    values = matrix.astype(jnp.float32)
    factor = lax.rsqrt(jnp.mean(values * values, axis=-1, keepdims=True) + 1e-06)
    return values * factor * gain


def causal_taps(mixed, filters):
    length = mixed.shape[-2]
    widths = [(0, 0)] * (mixed.ndim - 2) + [(2, 0), (0, 0)]
    padded = jnp.pad(mixed, widths)
    return (
        filters[0] * padded[..., 0:length, :]
        + filters[1] * padded[..., 1 : length + 1, :]
        + filters[2] * padded[..., 2 : length + 2, :]
    )


def gather_rows(normed):
    return lax.all_gather(normed, "tp", axis=0, tiled=True)


def project_in(gathered, stacked):
    return jnp.einsum(
        "td,kdc->ktc",
        gathered,
        lax.all_gather(stacked, "fs", axis=1, tiled=True),
        preferred_element_type=jnp.float32,
    )


def collect_out(weight):
    return lax.all_gather(weight, "fs", axis=1, tiled=True)


def sum_parts(local_cols, weight):
    return lax.psum_scatter(
        jnp.dot(local_cols, weight, preferred_element_type=jnp.float32).astype(jnp.bfloat16),
        "tp",
        scatter_dimension=0,
        tiled=True,
    ).astype(jnp.float32)


def on_device(
    tokens, mix_gain, w_bgate, w_cgate, w_value, conv_taps, w_mixout, mlp_gain, w_gate, w_up, w_down
):
    normed = rms_scale(tokens, mix_gain).astype(jnp.bfloat16)
    gathered = gather_rows(normed)
    projected = project_in(gathered, jnp.stack([w_bgate, w_cgate, w_value])).astype(jnp.bfloat16)
    channels = projected.shape[2]
    channel_taps = lax.dynamic_slice_in_dim(conv_taps, lax.axis_index("tp") * channels, channels, 1)
    mixed_in = projected[1].astype(jnp.float32) * projected[2].astype(jnp.float32)
    gated = (projected[0].astype(jnp.float32) * causal_taps(mixed_in, channel_taps)).astype(
        jnp.bfloat16
    )
    residual = tokens.astype(jnp.float32) + sum_parts(gated, collect_out(w_mixout))
    normed_two = rms_scale(residual, mlp_gain).astype(jnp.bfloat16)
    gathered_two = gather_rows(normed_two)
    gate_up = project_in(gathered_two, jnp.stack([w_gate, w_up]))
    hidden = (jax.nn.silu(gate_up[0]) * gate_up[1]).astype(jnp.bfloat16)
    result = residual + 0.5 * sum_parts(hidden, collect_out(w_down))
    return result.astype(jnp.bfloat16)


def solution(mesh):
    return jax.shard_map(
        on_device,
        mesh=mesh,
        in_specs=(
            P(("rep", "fs", "tp"), None),
            P(),
            P("fs", "tp"),
            P("fs", "tp"),
            P("fs", "tp"),
            P(),
            P("tp", "fs"),
            P(),
            P("fs", "tp"),
            P("fs", "tp"),
            P("tp", "fs"),
        ),
        out_specs=P(("rep", "fs", "tp"), None),
        check_vma=False,
    )
```

profile of v0, /device:TPU:0, one launch (start us, length us, event | category | flops | bytes accessed | tf_op | source)
XLA Modules:
  0.0 599.1 jit_solution(9736600943579483417)
XLA Ops:
  6.5 0.0 all-gather.9.cloned.1.call-start
  6.5 1.8 fusion.2
  8.3 2.7 fusion.4
  11.1 0.0 all-gather.9.cloned.1.call-update
  11.1 0.0 all-gather.7.cloned.1.call-start
  11.2 0.0 copy-done.5
  11.2 0.0 copy-done.6
  11.2 0.0 copy-done.7
  11.2 1.3 pad_maximum_fusion
  12.5 0.0 all-gather.7.cloned.1.call-update
  12.5 0.0 all-gather.11.cloned.1.call-start
  12.6 0.7 all-gather.11.cloned.1.call-update
  13.3 0.0 reduce-scatter.3.cloned.1.call-start
  13.3 0.9 constant_dynamic-slice_fusion
  14.2 11.1 %all-gather.9.cloned.1.call-done = bf16[640,2048]{1,0:T(8,128)(2,1)} async-done(((bf16[320,2048]{1,0:T(8,128)(2,1)}), bf16[640,2048]{1,0:T(8,128)(2,1)}) %all-gather.9.cloned.1.call-update) | async-done | bytes 2621456 | tf_op jit(solution)/shard_map/all_gather | solution.py:25
  25.3 179.5 %all-gather.7.cloned.1.call-done = bf16[3,2048,1024]{2,1,0:T(8,128)(2,1)} async-done(((bf16[3,256,1024]{2,1,0:T(8,128)(2,1)}), bf16[3,2048,1024]{2,1,0:T(8,128)(2,1)}) %all-gather.7.cloned.1.call-update) | async-done | bytes 12582928 | tf_op jit(solution)/shard_map/all_gather | solution.py:32
  204.8 12.0 %convert_bitcast_fusion = bf16[3,640,1024]{2,1,0:T(8,128)(2,1)S(1)} fusion(bf16[3,2048,1024]{2,1,0:T(8,128)(2,1)} %all-gather.7.cloned.1.call-done, bf16[640,2048]{1,0:T(8,128)(2,1)} %all-gather.9.cloned.1.call-done), kind=kOutput, calls=%fused_computation.1 | convolution fusion | flops 8055029760 | bytes 19136512 | tf_op jit(solution)/shard_map/td,kdc->ktc/dot_general | solution.py:29
  216.9 0.0 copy-start.2
  216.9 1.9 copy-done.2
  218.7 0.5 multiply_bitcast_fusion
  219.2 60.5 %all-gather.11.cloned.1.call-done = bf16[1024,2048]{1,0:T(8,128)(2,1)} async-done(((bf16[1024,256]{1,0:T(8,128)(2,1)}), bf16[1024,2048]{1,0:T(8,128)(2,1)}) %all-gather.11.cloned.1.call-update) | async-done | bytes 4194320 | tf_op jit(solution)/shard_map/all_gather | solution.py:38
  279.7 7.4 %convolution_convert_fusion.1 = bf16[640,2048]{1,0:T(8,128)(2,1)} fusion(bf16[1024,2048]{1,0:T(8,128)(2,1)} %all-gather.11.cloned.1.call-done, f32[640,1024]{1,0:T(8,128)S(1)} %multiply_bitcast_fusion, bf16[3,640,1024]{2,1,0:T(8,128)(2,1)} %copy-done.2, f32[1024]{0:T(1024)S(1)} %bitcast.51, f32[1024]{0:T(1024)S(1)} %bitcast.50, f32[1024]{0:T(1024)S(1)} %bitcast.49), kind=kOutput, calls=%fused_computation.10 | convolution fusion | flops 2690908160 | bytes 10760192 | tf_op jit(solution)/shard_map/dot_general | solution.py:43
  287.1 0.0 reduce-scatter.3.cloned.1.call-update
  287.1 0.0 all-gather.13.cloned.1.call-start
  287.2 1.0 copy-done.3
  288.2 0.3 copy.12
  288.5 0.0 copy-done.4
  288.5 0.0 copy-start
  288.5 0.3 copy.13
  288.8 1.3 pad_maximum_fusion.1
  290.1 0.0 all-gather.13.cloned.1.call-update
  290.1 0.0 all-gather.15.cloned.1.call-start
  290.2 5.7 reduce-scatter.3.cloned.1.call-done
  295.9 1.9 multiply_reduce_fusion
  297.9 0.0 copy-done.1
  297.9 1.6 multiply_convert_fusion
  299.5 0.0 all-gather.15.cloned.1.call-update
  299.5 0.0 all-gather.17.cloned.1.call-start
  299.6 0.7 all-gather.17.cloned.1.call-update
  300.3 0.2 reduce-scatter.5.cloned.1.call-start
  300.5 161.9 %all-gather.13.cloned.1.call-done = bf16[2,2048,1408]{1,2,0:T(8,128)(2,1)} async-done(((bf16[2,256,1408]{1,2,0:T(8,128)(2,1)}), bf16[2,2048,1408]{1,2,0:T(8,128)(2,1)}) %all-gather.13.cloned.1.call-update) | async-done | bytes 11534352 | tf_op jit(solution)/shard_map/all_gather | solution.py:32
  462.4 11.0 %all-gather.15.cloned.1.call-done = bf16[640,2048]{1,0:T(8,128)(2,1)} async-done(((bf16[320,2048]{1,0:T(8,128)(2,1)}), bf16[640,2048]{1,0:T(8,128)(2,1)}) %all-gather.15.cloned.1.call-update) | async-done | bytes 2621456 | tf_op jit(solution)/shard_map/all_gather | solution.py:25
  473.4 14.6 %convolution_bitcast_fusion = f32[2,640,1408]{1,2,0:T(8,128)} fusion(bf16[2,2048,1408]{1,2,0:T(8,128)(2,1)} %all-gather.13.cloned.1.call-done, bf16[640,2048]{1,0:T(8,128)(2,1)} %all-gather.15.cloned.1.call-done), kind=kOutput, calls=%fused_computation | convolution fusion | flops 7381975040 | bytes 21364736 | tf_op jit(solution)/shard_map/td,kdc->ktc/dot_general | solution.py:29
  488.0 81.8 %all-gather.17.cloned.1.call-done = bf16[1408,2048]{1,0:T(8,128)(2,1)} async-done(((bf16[1408,256]{1,0:T(8,128)(2,1)}), bf16[1408,2048]{1,0:T(8,128)(2,1)}) %all-gather.17.cloned.1.call-update) | async-done | bytes 5767184 | tf_op jit(solution)/shard_map/all_gather | solution.py:38
  569.8 10.7 %convolution_convert_fusion = bf16[640,2048]{1,0:T(8,128)(2,1)} fusion(bf16[1408,2048]{1,0:T(8,128)(2,1)} %all-gather.17.cloned.1.call-done, f32[2,640,1408]{1,2,0:T(8,128)} %convolution_bitcast_fusion), kind=kOutput, calls=%fused_computation.9 | convolution fusion | flops 3697704960 | bytes 15597568 | tf_op jit(solution)/shard_map/dot_general | solution.py:43
  580.4 0.0 reduce-scatter.5.cloned.1.call-update
  580.5 8.8 %reduce-scatter.5.cloned.1.call-done = bf16[320,2048]{1,0:T(8,128)(2,1)} async-done(((bf16[640,2048]{1,0:T(8,128)(2,1)}), bf16[320,2048]{1,0:T(8,128)(2,1)}) %reduce-scatter.5.cloned.1.call-update) | async-done | bytes 1310736 | tf_op jit(solution)/shard_map/reduce_scatter | solution.py:42
  589.3 3.1 add_convert_fusion
  (11 shorter events, 0.0 us)
Async XLA Ops:
  6.5 18.8 %all-gather.9.cloned.1.call-start = ((), (), s32[]{:S(2)}) async-start(), calls=%async_computation.3 | async-start | bytes 3932160 | tf_op jit(solution)/shard_map/all_gather | solution.py:25
  6.5 4.6 copy-start.5
  6.5 4.6 copy-start.6
  6.5 4.6 copy-start.7
  11.1 193.7 %all-gather.7.cloned.1.call-start = ((), (), s32[]{:S(2)}) async-start(), calls=%async_computation.2 | async-start | bytes 14155776 | tf_op jit(solution)/shard_map/all_gather | solution.py:32
  12.5 267.2 %all-gather.11.cloned.1.call-start = ((), (), s32[]{:S(2)}) async-start(), calls=%async_computation.4 | async-start | bytes 4718592 | tf_op jit(solution)/shard_map/all_gather | solution.py:38
  13.3 282.6 %reduce-scatter.3.cloned.1.call-start = ((), (), s32[]{:S(2)}) async-start(), calls=%async_computation.5 | async-start | bytes 3932160 | tf_op jit(solution)/shard_map/reduce_scatter | solution.py:42
  216.9 1.9 copy-start.2
  287.1 1.1 copy-start.3
  287.1 1.4 copy-start.4
  287.1 175.3 %all-gather.13.cloned.1.call-start = ((), (), s32[]{:S(2)}) async-start(), calls=%async_computation.6 | async-start | bytes 12976128 | tf_op jit(solution)/shard_map/all_gather | solution.py:32
  288.5 7.4 %copy-start = (bf16[320,2048]{1,0:T(8,128)(2,1)S(1)}, bf16[320,2048]{1,0:T(8,128)(2,1)}, u32[]{:S(2)}) copy-start(bf16[320,2048]{1,0:T(8,128)(2,1)} %param.11) | copy-start | bytes 3932164
  290.1 7.8 %copy-start.8 = (f32[2048]{0:T(1024)S(1)}, f32[2048]{0:T(1024)}, u32[]{:S(2)}) copy-start(f32[2048]{0:T(1024)} %param.18) | copy-start | bytes 24580
  290.1 183.3 %all-gather.15.cloned.1.call-start = ((), (), s32[]{:S(2)}) async-start(), calls=%async_computation.7 | async-start | bytes 3932160 | tf_op jit(solution)/shard_map/all_gather | solution.py:25
  295.9 2.0 copy-start.1
  299.5 270.3 %all-gather.17.cloned.1.call-start = ((), (), s32[]{:S(2)}) async-start(), calls=%async_computation.8 | async-start | bytes 6488064 | tf_op jit(solution)/shard_map/all_gather | solution.py:38
  300.3 289.0 %reduce-scatter.5.cloned.1.call-start = ((), (), s32[]{:S(2)}) async-start(), calls=%async_computation.9 | async-start | bytes 3932160 | tf_op jit(solution)/shard_map/reduce_scatter | solution.py:42
Sparse Core Ops, SparseCore 0:
  11.2 14.0 all-gather.8
  27.5 177.2 all-gather.6
  206.9 72.7 all-gather.10
  287.2 8.6 reduce-scatter.2
  297.8 164.5 all-gather.12
  463.8 9.5 all-gather.14
  475.4 94.3 all-gather.16
  580.6 8.6 reduce-scatter.4
where the time goes:
time: 599 us
  waiting for transfers between devices  522 us (87%)
  matrix products  44.7 us (7%)
  other arithmetic  14.3 us (2%)
  between operations  13.6 us (2%)
    all_gather x2, waiting for transfers between devices, project_in(): lax.all_gather(stacked, 'fs', axis=1, tiled=True)  341 us
    all_gather x2, waiting for transfers between devices, collect_out(): return lax.all_gather(weight, 'fs', axis=1, tiled=True)  142 us
    dot_general x2, matrix products, project_in(): jnp.einsum('td,kdc->ktc', gathered, lax.all_gather(stacked, 'fs', axis=1,...  26.7 us
    all_gather x2, waiting for transfers between devices, gather_rows(): return lax.all_gather(normed, 'tp', axis=0, tiled=True)  22 us
    dot_general x2, matrix products, sum_parts(): jnp.dot(local_cols, weight, preferred_element_type=jnp.float32)  18 us
    reduce_scatter x2, waiting for transfers between devices, sum_parts(): lax.psum_scatter(jnp.dot(local_cols, weight, preferred_element_type=jnp.f...  14.5 us
  transfers between devices with their start and end apart: 8, of which 8 were waited for; matrix products, arithmetic and copies ran while one was open for 6% of the time, Pallas kernels for 0%

commit v1 on v0

--- a/solution.py
+++ b/solution.py
@@ -2,6 +2,22 @@
 import jax.numpy as jnp
 from jax import lax
 from jax.sharding import PartitionSpec as P
+
+
+def product_in_turn(x, axis, dim, product):
+    size, position, span = (lax.axis_size(axis), lax.axis_index(axis), x.shape[dim])
+    ahead = [(i, (i + 1) % size) for i in range(size)]
+    downward = [(i, (i - 1) % size) for i in range(size)]
+    half = size // 2
+    from_left = from_right = x
+    so_far = product(x, position * span)
+    for step in range(1, half + 1):
+        from_left = lax.ppermute(from_left, axis, ahead)
+        if step < size - half:
+            from_right = lax.ppermute(from_right, axis, downward)
+            so_far = so_far + product(from_right, (position + step) % size * span)
+        so_far = so_far + product(from_left, (position - step) % size * span)
+    return so_far
 
 
 def rms_scale(matrix, gain):
@@ -26,11 +42,16 @@
 
 
 def project_in(gathered, stacked):
-    return jnp.einsum(
-        "td,kdc->ktc",
-        gathered,
-        lax.all_gather(stacked, "fs", axis=1, tiled=True),
-        preferred_element_type=jnp.float32,
+    return product_in_turn(
+        stacked,
+        "fs",
+        1,
+        lambda shard, start: jnp.einsum(
+            "td,kdc->ktc",
+            lax.dynamic_slice_in_dim(gathered, start, shard.shape[1], axis=1),
+            shard,
+            preferred_element_type=jnp.float32,
+        ),
     )
 
 

time: 599 us -> 656 us (1.095)
  matrix products: 44.7 us -> 127 us
  waiting for transfers between devices: 522 us -> 456 us
  starting transfers between devices: 0.47 us -> 35 us
    ppermute x0 -> x14, waiting for transfers between devices: none -> 437 us  [the longest x8 423 us: product_in_turn(): from_left = lax.ppermute(from_left, axis, ahead)]
    all_gather x2 -> x0, waiting for transfers between devices: 341 us -> none  [project_in(): lax.all_gather(stacked, 'fs', axis=1, tiled=True)]
    all_gather x2, waiting for transfers between devices: 142 us -> 0.01 us  [collect_out(): return lax.all_gather(weight, 'fs', axis=1, tiled=True)]
    dot_general x2 -> x16, matrix products: 26.7 us -> 106 us  [project_in(): jnp.einsum('td,kdc->ktc', lax.dynamic_slice_in_dim(gathered, start, shard...]
    ppermute x0 -> x14, starting transfers between devices: none -> 34.8 us  [the longest x8 19.9 us: product_in_turn(): from_left = lax.ppermute(from_left, axis, ahead)]
    all_gather x2, waiting for transfers between devices: 22 us -> 0.02 us  [gather_rows(): return lax.all_gather(normed, 'tp', axis=0, tiled=True)]
  transfers between devices with their start and end apart: 8 -> 20, of which waited for: 8 -> 11; matrix products, arithmetic and copies ran while one was open for 6% -> 18% of each run, Pallas kernels for 0% -> 0%
where the time goes in v1:
time: 656 us; the launch traced here: 655 us
  waiting for transfers between devices  456 us (70%)
  matrix products  127 us (19%)
  starting transfers between devices  35 us (5%)
  other arithmetic  15.8 us (2%)
  between operations  13.6 us (2%)
  local copies, waits for them, and re-layouts  7.58 us (1%)
    ppermute x8, waiting for transfers between devices, product_in_turn(): from_left = lax.ppermute(from_left, axis, ahead)  423 us
    dot_general x16, matrix products, project_in(): jnp.einsum('td,kdc->ktc', lax.dynamic_slice_in_dim(gathered, start, shard...  106 us
    dot_general x2, matrix products, sum_parts(): jnp.dot(local_cols, weight, preferred_element_type=jnp.float32)  20.6 us
    ppermute x8, starting transfers between devices, product_in_turn(): from_left = lax.ppermute(from_left, axis, ahead)  19.9 us
    reduce_scatter x2, waiting for transfers between devices, sum_parts(): lax.psum_scatter(jnp.dot(local_cols, weight, preferred_element_type=jnp.f...  18.2 us
    ppermute x6, starting transfers between devices, product_in_turn(): from_right = lax.ppermute(from_right, axis, downward)  14.9 us
    ppermute x6, waiting for transfers between devices, product_in_turn(): from_right = lax.ppermute(from_right, axis, downward)  14.6 us
  transfers between devices with their start and end apart: 20, of which 11 were waited for; matrix products, arithmetic and copies ran while one was open for 18% of the time, Pallas kernels for 0%

profile of v1, /device:TPU:0, one launch (start us, length us, event | category | flops | bytes accessed | tf_op | source)
XLA Modules:
  0.0 655.1 jit_solution(10982762843762781919)
XLA Ops:
  8.3 2.7 fusion.5
  12.6 3.0 collective-permute-start.1
  15.6 3.0 collective-permute-start
  18.6 64.6 %collective-permute-done.1 = bf16[3,256,1024]{2,1,0:T(8,128)(2,1)S(1)} collective-permute-done((bf16[3,256,1024]{2,1,0:T(8,128)(2,1)}, bf16[3,256,1024]{2,1,0:T(8,128)(2,1)S(1)}, u32[]{:S(2)}, u32[]{:S(2)}) %collective-permute-start.1) | collective-permute-done | bytes 1572896 | tf_op jit(solution)/shard_map/ppermute | solution.py:15
  83.2 2.4 collective-permute-start.3
  85.7 3.1 collective-permute-start.2
  88.8 76.0 %collective-permute-done.3 = bf16[3,256,1024]{2,1,0:T(8,128)(2,1)S(1)} collective-permute-done((bf16[3,256,1024]{2,1,0:T(8,128)(2,1)S(1)}, bf16[3,256,1024]{2,1,0:T(8,128)(2,1)S(1)}, u32[]{:S(2)}, u32[]{:S(2)}) %collective-permute-start.3) | collective-permute-done | bytes 1572896 | tf_op jit(solution)/shard_map/ppermute | solution.py:15
  164.8 2.5 collective-permute-start.5
  168.2 2.3 fusion.37
  170.6 5.8 fusion.39
  176.4 3.1 collective-permute-start.4
  179.5 4.3 fusion.41
  183.8 63.8 %collective-permute-done.5 = bf16[3,256,1024]{2,1,0:T(8,128)(2,1)} collective-permute-done((bf16[3,256,1024]{2,1,0:T(8,128)(2,1)S(1)}, bf16[3,256,1024]{2,1,0:T(8,128)(2,1)}, u32[]{:S(2)}, u32[]{:S(2)}) %collective-permute-start.5) | collective-permute-done | bytes 1572896 | tf_op jit(solution)/shard_map/ppermute | solution.py:15
  247.6 2.6 collective-permute-start.6
  250.2 4.3 fusion.33
  254.5 5.8 fusion.35
  260.3 5.7 fusion.29
  266.0 4.4 fusion.31
  270.3 15.7 %collective-permute-done.6 = bf16[3,256,1024]{2,1,0:T(8,128)(2,1)} collective-permute-done((bf16[3,256,1024]{2,1,0:T(8,128)(2,1)}, bf16[3,256,1024]{2,1,0:T(8,128)(2,1)}, u32[]{:S(2)}, u32[]{:S(2)}) %collective-permute-start.6) | collective-permute-done | bytes 1572896 | tf_op jit(solution)/shard_map/ppermute | solution.py:15
  286.0 16.3 %fusion = bf16[3,640,1024]{2,1,0:T(8,128)(2,1)S(1)} fusion(f32[3,1024,640]{1,2,0:T(8,128)} %fusion.29, f32[3,1024,640]{1,2,0:T(8,128)} %fusion.31, f32[3,1024,640]{1,2,0:T(8,128)} %fusion.33, f32[3,1024,640]{1,2,0:T(8,128)} %fusion.35, f32[3,1024,640]{1,2,0:T(8,128)S(1)} %fusion.37, f32[3,1024,640]{1,2,0:T(8,128)} %fusion.41, f32[3,1024,640]{1,2,0:T(8,128)} %fusion.39, ...), kind=kOutput, calls=%fused_computation.2 | convolution fusion | flops 1022361600 | bytes 60882948 | tf_op jit(solution)/shard_map/td,kdc->ktc/dot_general | solution.py:49
  302.3 1.8 copy-done.2
  304.2 2.1 multiply_bitcast_fusion
  306.2 9.7 %convolution_convert_fusion.1 = bf16[640,2048]{1,0:T(8,128)(2,1)} fusion(bf16[1024,2048]{1,0:T(8,128)(2,1)} %all-gather.7.cloned.1.call-done, f32[640,1024]{1,0:T(8,128)} %multiply_bitcast_fusion, bf16[3,640,1024]{2,1,0:T(8,128)(2,1)} %copy-done.2, f32[1024]{0:T(1024)S(1)} %bitcast.108, f32[1024]{0:T(1024)S(1)} %bitcast.107, f32[1024]{0:T(1024)S(1)} %bitcast.106), kind=kOutput, calls=%fused_computation.11 | convolution fusion | flops 2690908160 | bytes 10760192 | tf_op jit(solution)/shard_map/dot_general | solution.py:64
  316.0 9.0 %reduce-scatter.3.cloned.1.call-done = bf16[320,2048]{1,0:T(8,128)(2,1)} async-done(((bf16[640,2048]{1,0:T(8,128)(2,1)}), bf16[320,2048]{1,0:T(8,128)(2,1)}) %reduce-scatter.3.cloned.1.call-update) | async-done | bytes 1310736 | tf_op jit(solution)/shard_map/reduce_scatter | solution.py:63
  325.0 1.9 multiply_reduce_fusion
  330.6 2.2 copy.13
  334.1 1.9 collective-permute-start.8
  336.0 2.9 collective-permute-start.7
  338.9 66.9 %collective-permute-done.8 = bf16[2,256,1408]{1,2,0:T(8,128)(2,1)S(1)} collective-permute-done((bf16[2,256,1408]{1,2,0:T(8,128)(2,1)S(1)}, bf16[2,256,1408]{1,2,0:T(8,128)(2,1)S(1)}, u32[]{:S(2)}, u32[]{:S(2)}) %collective-permute-start.8) | collective-permute-done | bytes 1441824 | tf_op jit(solution)/shard_map/ppermute | solution.py:15
  405.8 2.5 collective-permute-start.10
  409.4 2.8 collective-permute-start.9
  412.2 88.0 %collective-permute-done.10 = bf16[2,256,1408]{1,2,0:T(8,128)(2,1)S(1)} collective-permute-done((bf16[2,256,1408]{1,2,0:T(8,128)(2,1)S(1)}, bf16[2,256,1408]{1,2,0:T(8,128)(2,1)S(1)}, u32[]{:S(2)}, u32[]{:S(2)}) %collective-permute-start.10) | collective-permute-done | bytes 1441824 | tf_op jit(solution)/shard_map/ppermute | solution.py:15
  500.2 2.5 collective-permute-start.12
  502.7 12.1 %collective-permute-done.9 = bf16[2,256,1408]{1,2,0:T(8,128)(2,1)} collective-permute-done((bf16[2,256,1408]{1,2,0:T(8,128)(2,1)S(1)}, bf16[2,256,1408]{1,2,0:T(8,128)(2,1)}, u32[]{:S(2)}, u32[]{:S(2)}) %collective-permute-start.9) | collective-permute-done | bytes 1441824 | tf_op jit(solution)/shard_map/ppermute | solution.py:17
  514.7 47.8 %collective-permute-done.12 = bf16[2,256,1408]{1,2,0:T(8,128)(2,1)} collective-permute-done((bf16[2,256,1408]{1,2,0:T(8,128)(2,1)S(1)}, bf16[2,256,1408]{1,2,0:T(8,128)(2,1)}, u32[]{:S(2)}, u32[]{:S(2)}) %collective-permute-start.12) | collective-permute-done | bytes 1441824 | tf_op jit(solution)/shard_map/ppermute | solution.py:15
  562.5 2.6 collective-permute-start.13
  565.1 5.8 fusion.18
  570.9 5.8 fusion.20
  576.7 4.2 fusion.22
  580.9 4.2 fusion.26
  585.2 4.3 fusion.24
  589.4 5.6 fusion.14
  595.0 2.6 collective-permute-done.11
  597.6 5.6 fusion.16
  603.2 21.8 %add_bitcast_fusion = f32[2,640,1408]{1,2,0:T(8,128)} fusion(f32[2,1408,640]{2,1,0:T(8,128)} %fusion.14, f32[2,1408,640]{2,1,0:T(8,128)} %fusion.16, f32[2,1408,640]{2,1,0:T(8,128)} %fusion.18, f32[2,1408,640]{2,1,0:T(8,128)} %fusion.20, f32[2,1408,640]{2,1,0:T(8,128)} %fusion.22, f32[2,1408,640]{2,1,0:T(8,128)} %fusion.26, f32[2,1408,640]{2,1,0:T(8,128)} %fusion.24, ...), kind=kOutput, calls=%fused_computation.1 | convolution fusion | flops 935362560 | bytes 59441156 | tf_op jit(solution)/shard_map/td,kdc->ktc/dot_general | solution.py:49
  625.0 10.9 %convolution_convert_fusion = bf16[640,2048]{1,0:T(8,128)(2,1)} fusion(bf16[1408,2048]{1,0:T(8,128)(2,1)} %all-gather.11.cloned.1.call-done, f32[2,640,1408]{1,2,0:T(8,128)} %add_bitcast_fusion), kind=kOutput, calls=%fused_computation.10 | convolution fusion | flops 3697704960 | bytes 15597568 | tf_op jit(solution)/shard_map/dot_general | solution.py:64
  636.0 9.2 %reduce-scatter.5.cloned.1.call-done = bf16[320,2048]{1,0:T(8,128)(2,1)} async-done(((bf16[640,2048]{1,0:T(8,128)(2,1)}), bf16[320,2048]{1,0:T(8,128)(2,1)}) %reduce-scatter.5.cloned.1.call-update) | async-done | bytes 1310736 | tf_op jit(solution)/shard_map/reduce_scatter | solution.py:63
  645.2 3.1 add_convert_fusion.1
  (65 shorter events, 10.4 us)
Async XLA Ops:
  6.5 4.6 copy-start.6
  6.5 4.6 copy-start.8
  6.5 4.6 copy-start.10
  6.5 161.7 %all-gather.5.cloned.1.call-start = ((), (), s32[]{:S(2)}) async-start(), calls=%async_computation.2 | async-start | bytes 3932160 | tf_op jit(solution)/shard_map/all_gather | solution.py:41
  11.1 295.1 %all-gather.7.cloned.1.call-start = ((), (), s32[]{:S(2)}) async-start(), calls=%async_computation.3 | async-start | bytes 4718592 | tf_op jit(solution)/shard_map/all_gather | solution.py:59
  12.6 70.7 %collective-permute-start.1 = (bf16[3,256,1024]{2,1,0:T(8,128)(2,1)}, bf16[3,256,1024]{2,1,0:T(8,128)(2,1)S(1)}, u32[]{:S(2)}, u32[]{:S(2)}) collective-permute-start(bf16[3,256,1024]{2,1,0:T(8,128)(2,1)} %pad_maximum_fusion), channel_id=1, source_target_pairs={{0,2},{2,4},{4,6},{6,8},{8,10},{10,12},{12,14},{14,0},{1,3},{3,5},... | collective-permute-start | bytes 4718600 | tf_op jit(solution)/shard_map/ppermute | solution.py:15
  15.6 70.1 %collective-permute-start = (bf16[3,256,1024]{2,1,0:T(8,128)(2,1)}, bf16[3,256,1024]{2,1,0:T(8,128)(2,1)}, u32[]{:S(2)}, u32[]{:S(2)}) collective-permute-start(bf16[3,256,1024]{2,1,0:T(8,128)(2,1)} %pad_maximum_fusion), channel_id=1, source_target_pairs={{0,14},{2,0},{4,2},{6,4},{8,6},{10,8},{12,10},{14,12},{1,15},{3,1}... | collective-permute-start | bytes 4718600 | tf_op jit(solution)/shard_map/ppermute | solution.py:17
  83.2 81.6 %collective-permute-start.3 = (bf16[3,256,1024]{2,1,0:T(8,128)(2,1)S(1)}, bf16[3,256,1024]{2,1,0:T(8,128)(2,1)S(1)}, u32[]{:S(2)}, u32[]{:S(2)}) collective-permute-start(bf16[3,256,1024]{2,1,0:T(8,128)(2,1)S(1)} %collective-permute-done.1), channel_id=1, source_target_pairs={{0,2},{2,4},{4,6},{6,8},{8,10},{10,12},{12,14},{14,0},{1,3},{3,5},... | collective-permute-start | bytes 4718600 | tf_op jit(solution)/shard_map/ppermute | solution.py:15
  85.6 239.3 %reduce-scatter.3.cloned.1.call-start = ((), (), s32[]{:S(2)}) async-start(), calls=%async_computation.4 | async-start | bytes 3932160 | tf_op jit(solution)/shard_map/reduce_scatter | solution.py:63
  85.7 90.7 %collective-permute-start.2 = (bf16[3,256,1024]{2,1,0:T(8,128)(2,1)}, bf16[3,256,1024]{2,1,0:T(8,128)(2,1)}, u32[]{:S(2)}, u32[]{:S(2)}) collective-permute-start(bf16[3,256,1024]{2,1,0:T(8,128)(2,1)} %collective-permute-done), channel_id=1, source_target_pairs={{0,14},{2,0},{4,2},{6,4},{8,6},{10,8},{12,10},{14,12},{1,15},{3,1}... | collective-permute-start | bytes 4718600 | tf_op jit(solution)/shard_map/ppermute | solution.py:17
  164.8 82.8 %collective-permute-start.5 = (bf16[3,256,1024]{2,1,0:T(8,128)(2,1)S(1)}, bf16[3,256,1024]{2,1,0:T(8,128)(2,1)}, u32[]{:S(2)}, u32[]{:S(2)}) collective-permute-start(bf16[3,256,1024]{2,1,0:T(8,128)(2,1)S(1)} %collective-permute-done.3), channel_id=1, source_target_pairs={{0,2},{2,4},{4,6},{6,8},{8,10},{10,12},{12,14},{14,0},{1,3},{3,5},... | collective-permute-start | bytes 4718600 | tf_op jit(solution)/shard_map/ppermute | solution.py:15
  168.2 2.3 copy-start.4
  170.5 8.9 %copy-start.7 = (bf16[256,1024]{1,0:T(8,128)(2,1)S(1)}, bf16[256,1024]{1,0:T(8,128)(2,1)}, u32[]{:S(2)}) copy-start(bf16[256,1024]{1,0:T(8,128)(2,1)} %param.15) | copy-start | bytes 1572868
  170.6 8.9 %copy-start.9 = (bf16[256,1024]{1,0:T(8,128)(2,1)S(1)}, bf16[256,1024]{1,0:T(8,128)(2,1)}, u32[]{:S(2)}) copy-start(bf16[256,1024]{1,0:T(8,128)(2,1)} %param.14) | copy-start | bytes 1572868
  170.6 8.9 %copy-start.11 = (bf16[256,1024]{1,0:T(8,128)(2,1)S(1)}, bf16[256,1024]{1,0:T(8,128)(2,1)}, u32[]{:S(2)}) copy-start(bf16[256,1024]{1,0:T(8,128)(2,1)} %param.13) | copy-start | bytes 1572868
  176.4 89.6 %collective-permute-start.4 = (bf16[3,256,1024]{2,1,0:T(8,128)(2,1)}, bf16[3,256,1024]{2,1,0:T(8,128)(2,1)S(1)}, u32[]{:S(2)}, u32[]{:S(2)}) collective-permute-start(bf16[3,256,1024]{2,1,0:T(8,128)(2,1)} %collective-permute-done.2), channel_id=1, source_target_pairs={{0,14},{2,0},{4,2},{6,4},{8,6},{10,8},{12,10},{14,12},{1,15},{3,1}... | collective-permute-start | bytes 4718600 | tf_op jit(solution)/shard_map/ppermute | solution.py:17
  247.6 38.4 %collective-permute-start.6 = (bf16[3,256,1024]{2,1,0:T(8,128)(2,1)}, bf16[3,256,1024]{2,1,0:T(8,128)(2,1)}, u32[]{:S(2)}, u32[]{:S(2)}) collective-permute-start(bf16[3,256,1024]{2,1,0:T(8,128)(2,1)} %collective-permute-done.5), channel_id=1, source_target_pairs={{0,2},{2,4},{4,6},{6,8},{8,10},{10,12},{12,14},{14,0},{1,3},{3,5},... | collective-permute-start | bytes 4718600 | tf_op jit(solution)/shard_map/ppermute | solution.py:15
  302.3 1.9 copy-start.2
  315.9 9.1 %copy-start = (bf16[320,2048]{1,0:T(8,128)(2,1)S(1)}, bf16[320,2048]{1,0:T(8,128)(2,1)}, u32[]{:S(2)}) copy-start(bf16[320,2048]{1,0:T(8,128)(2,1)} %param.11) | copy-start | bytes 3932164
  315.9 11.0 %copy-start.17 = (f32[2048]{0:T(1024)S(1)}, f32[2048]{0:T(1024)}, u32[]{:S(2)}) copy-start(f32[2048]{0:T(1024)} %param.18) | copy-start | bytes 24580
  315.9 249.2 %all-gather.9.cloned.1.call-start = ((), (), s32[]{:S(2)}) async-start(), calls=%async_computation.5 | async-start | bytes 3932160 | tf_op jit(solution)/shard_map/all_gather | solution.py:41
  325.0 2.0 copy-start.1
  328.6 296.4 %all-gather.11.cloned.1.call-start = ((), (), s32[]{:S(2)}) async-start(), calls=%async_computation.6 | async-start | bytes 6488064 | tf_op jit(solution)/shard_map/all_gather | solution.py:59
  329.2 316.0 %reduce-scatter.5.cloned.1.call-start = ((), (), s32[]{:S(2)}) async-start(), calls=%async_computation.7 | async-start | bytes 3932160 | tf_op jit(solution)/shard_map/reduce_scatter | solution.py:63
  334.1 71.7 %collective-permute-start.8 = (bf16[2,256,1408]{1,2,0:T(8,128)(2,1)S(1)}, bf16[2,256,1408]{1,2,0:T(8,128)(2,1)S(1)}, u32[]{:S(2)}, u32[]{:S(2)}) collective-permute-start(bf16[2,256,1408]{1,2,0:T(8,128)(2,1)S(1)} %pad_maximum_fusion.1), channel_id=1, source_target_pairs={{0,2},{2,4},{4,6},{6,8},{8,10},{10,12},{12,14},{14,0},{1,3},{3,5},... | collective-permute-start | bytes 4325384 | tf_op jit(solution)/shard_map/ppermute | solution.py:15
  336.0 72.3 %collective-permute-start.7 = (bf16[2,256,1408]{1,2,0:T(8,128)(2,1)S(1)}, bf16[2,256,1408]{1,2,0:T(8,128)(2,1)S(1)}, u32[]{:S(2)}, u32[]{:S(2)}) collective-permute-start(bf16[2,256,1408]{1,2,0:T(8,128)(2,1)S(1)} %pad_maximum_fusion.1), channel_id=1, source_target_pairs={{0,14},{2,0},{4,2},{6,4},{8,6},{10,8},{12,10},{14,12},{1,15},{3,1}... | collective-permute-start | bytes 4325384 | tf_op jit(solution)/shard_map/ppermute | solution.py:17
  405.8 108.9 %copy-start.14 = (bf16[2,256,1408]{1,2,0:T(8,128)(2,1)}, bf16[2,256,1408]{1,2,0:T(8,128)(2,1)S(1)}, u32[]{:S(2)}) copy-start(bf16[2,256,1408]{1,2,0:T(8,128)(2,1)S(1)} %collective-permute-done.8) | copy-start | bytes 4325380
  405.8 94.4 %collective-permute-start.10 = (bf16[2,256,1408]{1,2,0:T(8,128)(2,1)S(1)}, bf16[2,256,1408]{1,2,0:T(8,128)(2,1)S(1)}, u32[]{:S(2)}, u32[]{:S(2)}) collective-permute-start(bf16[2,256,1408]{1,2,0:T(8,128)(2,1)S(1)} %collective-permute-done.8), channel_id=1, source_target_pairs={{0,2},{2,4},{4,6},{6,8},{8,10},{10,12},{12,14},{14,0},{1,3},{3,5},... | collective-permute-start | bytes 4325384 | tf_op jit(solution)/shard_map/ppermute | solution.py:15
  408.3 1.1 copy-start.12
  409.4 105.3 %collective-permute-start.9 = (bf16[2,256,1408]{1,2,0:T(8,128)(2,1)S(1)}, bf16[2,256,1408]{1,2,0:T(8,128)(2,1)}, u32[]{:S(2)}, u32[]{:S(2)}) collective-permute-start(bf16[2,256,1408]{1,2,0:T(8,128)(2,1)S(1)} %collective-permute-done.7), channel_id=1, source_target_pairs={{0,14},{2,0},{4,2},{6,4},{8,6},{10,8},{12,10},{14,12},{1,15},{3,1}... | collective-permute-start | bytes 4325384 | tf_op jit(solution)/shard_map/ppermute | solution.py:17
  500.2 14.5 %copy-start.16 = (bf16[2,256,1408]{1,2,0:T(8,128)(2,1)}, bf16[2,256,1408]{1,2,0:T(8,128)(2,1)S(1)}, u32[]{:S(2)}) copy-start(bf16[2,256,1408]{1,2,0:T(8,128)(2,1)S(1)} %collective-permute-done.10) | copy-start | bytes 4325380
  500.2 62.3 %collective-permute-start.12 = (bf16[2,256,1408]{1,2,0:T(8,128)(2,1)S(1)}, bf16[2,256,1408]{1,2,0:T(8,128)(2,1)}, u32[]{:S(2)}, u32[]{:S(2)}) collective-permute-start(bf16[2,256,1408]{1,2,0:T(8,128)(2,1)S(1)} %collective-permute-done.10), channel_id=1, source_target_pairs={{0,2},{2,4},{4,6},{6,8},{8,10},{10,12},{12,14},{14,0},{1,3},{3,5},... | collective-permute-start | bytes 4325384 | tf_op jit(solution)/shard_map/ppermute | solution.py:15
  514.7 82.8 %collective-permute-start.11 = (bf16[2,256,1408]{1,2,0:T(8,128)(2,1)}, bf16[2,256,1408]{1,2,0:T(8,128)(2,1)}, u32[]{:S(2)}, u32[]{:S(2)}) collective-permute-start(bf16[2,256,1408]{1,2,0:T(8,128)(2,1)} %collective-permute-done.9), channel_id=1, source_target_pairs={{0,14},{2,0},{4,2},{6,4},{8,6},{10,8},{12,10},{14,12},{1,15},{3,1}... | collective-permute-start | bytes 4325384 | tf_op jit(solution)/shard_map/ppermute | solution.py:17
  562.5 40.7 %collective-permute-start.13 = (bf16[2,256,1408]{1,2,0:T(8,128)(2,1)}, bf16[2,256,1408]{1,2,0:T(8,128)(2,1)}, u32[]{:S(2)}, u32[]{:S(2)}) collective-permute-start(bf16[2,256,1408]{1,2,0:T(8,128)(2,1)} %collective-permute-done.12), channel_id=1, source_target_pairs={{0,2},{2,4},{4,6},{6,8},{8,10},{10,12},{12,14},{14,0},{1,3},{3,5},... | collective-permute-start | bytes 4325384 | tf_op jit(solution)/shard_map/ppermute | solution.py:15
  565.1 5.8 copy-start.5
  570.9 5.8 copy-start.15
  576.7 4.2 copy-start.3
  580.9 4.3 copy-start.13
Sparse Core Ops, SparseCore 0:
  11.2 14.0 all-gather.4
  85.8 155.2 all-gather.6
  316.0 8.8 reduce-scatter.2
  328.7 12.6 all-gather.8
  343.3 203.4 all-gather.10
  636.1 9.0 reduce-scatter.4
